TPU v7x, 32 devices: a whole 2x2x4 slice. The times are simulated.
32 devices in a mesh: grp: 2 (over y), ep: 4 (over z), tp: 4 (over x, core).
Axes of the slice: x: 2, y: 2, z: 4, core: 2. Of those that a mesh axis runs over, the one named last changes fastest.
Arguments:
- hidden_in: bfloat16 [4096, 2048], P(('grp', 'ep', 'tp')), parts along dimension 0, may hold values from -6 to 6
- expert_ids: int32 [4096, 2], P(('grp', 'ep', 'tp')), parts along dimension 0, may hold values from 0 to 15, all different within a row; in each aligned block of 128 rows (0 to 127, 128 to 255, ...) at most 32 rows name the same one
- route_weights: float32 [4096, 2], P(('grp', 'ep', 'tp')), parts along dimension 0, may hold values from 0.1 to 1
- norm_gain: float32 [2048], replicated, may hold values from 0.1 to 1.9
- gate_proj: bfloat16 [16, 2048, 512], P(('ep', 'tp')), may hold values from -0.125 to 0.125
- up_proj: bfloat16 [16, 2048, 512], P(('ep', 'tp')), may hold values from -0.125 to 0.125
- down_proj: bfloat16 [16, 512, 2048], P(('ep', 'tp')), may hold values from -0.25 to 0.25
Outputs:
- mixed_out: bfloat16 [4096, 2048], P(('grp', 'ep', 'tp')), parts along dimension 0
There are 2 independent parts, one for each index of `grp`. A program takes and returns all parts, laid end to end along the dimension named above; an argument that names none is the same for every part. Nothing has to cross between parts.
Inputs may be any that keep to these rules, and one draw needn't show every extreme that they name: `expert_ids`: each token names 2 different experts; among the 128 tokens of one device (aligned blocks of rows) no expert is named more than 32 times, and in every draw some expert is named exactly 32 times by some device's tokens.
All inputs are finite; a program needn't handle non-finite values.
Results may differ from a plain program's by a relative error of at most 0.0071.
Values may be sent and summed in bfloat16 or wider, within the bound.
A program may use at most 64 MiB of HBM per device.

v0:
```python
import functools

import jax
import jax.numpy as jnp
from jax import lax
from jax.experimental import pallas as pl
from jax.experimental.pallas import tpu as pltpu
from jax.sharding import PartitionSpec as P

Z_CHUNKS = 2
X_CHUNKS = 1


def slot_capacity(choose_count, token_count, expert_count):
    return max(2, 2 * choose_count * token_count // expert_count)


def pick(z, table):
    value = jnp.int32(table[0])
    for index in range(1, len(table)):
        value = jnp.where(z == index, jnp.int32(table[index]), value)
    return value


def kernel(
    n, m, cap, chunks, xchunks,
    hid, ids, wts, gain, gate_hbm, up_hbm, down_hbm, out,
    ag, meta, disp, xin, res, back, part, rin_l, rin_r, acc, gate, up, down,
    w_sem, ag_s, ag_r, me_s, me_r, xd_s, xd_r, xb_s, xb_r, rs_s, rs_l, rs_r,
):
    z = lax.axis_index("ep")
    t = lax.axis_index("tp")
    tokens, width = hid.shape
    rows = m * cap
    cw = width // chunks
    xw = width // xchunks
    ratio = chunks // xchunks
    choose = ids.shape[0]
    experts = n * m
    middle = jnp.logical_and(z > 0, z < n - 1)
    end = jnp.logical_or(z == 0, z == n - 1)
    by_z = [sorted(range(n), key=lambda b: (abs(b - q), b)) for q in range(n)]
    order = [pick(z, [by_z[q][s] for q in range(n)]) for s in range(n)]

    def to_ep(q):
        return {"ep": q}

    def to_tp(q):
        return {"tp": q}

    def cols(c):
        return pl.ds(c * cw, cw)

    def xcols(q):
        return pl.ds(q * xw, xw)

    loads = [
        pltpu.make_async_copy(gate_hbm.at[0], gate, w_sem.at[0]),
        pltpu.make_async_copy(up_hbm.at[0], up, w_sem.at[1]),
        pltpu.make_async_copy(down_hbm.at[0], down, w_sem.at[2]),
    ]
    for load in loads:
        load.start()

    barrier = pltpu.get_barrier_semaphore()

    def greet(q):
        pl.semaphore_signal(
            barrier, inc=1, device_id=q, device_id_type=pl.DeviceIdType.MESH
        )

    for d in range(1, m):
        greet(to_tp(lax.rem(t + d, m)))

    @pl.when(z > 0)
    def _():
        greet(to_ep(z - 1))

    @pl.when(z < n - 1)
    def _():
        greet(to_ep(z + 1))

    def remote(src, dst, s_sem, r_sem, dev):
        return pltpu.make_async_remote_copy(
            src_ref=src, dst_ref=dst, send_sem=s_sem, recv_sem=r_sem,
            device_id=dev, device_id_type=pl.DeviceIdType.MESH,
        )

    right, left = jnp.minimum(z + 1, n - 1), jnp.maximum(z - 1, 0)

    def ag_copy(b, c, side):
        return remote(
            ag.at[b, c], ag.at[b, c], ag_s.at[side, b, c], ag_r.at[b, c],
            to_ep(left if side == 0 else right),
        )

    def me_copy(b, side):
        return remote(
            meta.at[b], meta.at[b], me_s.at[side, b], me_r.at[b],
            to_ep(left if side == 0 else right),
        )

    def xd_copy(b, j, c):
        return remote(
            disp.at[b, c, j], xin.at[b, c, t], xd_s.at[b, j, c],
            xd_r.at[b, t, c], to_tp(j),
        )

    def xd_from(b, j, c):
        return remote(
            disp.at[b, c, j], xin.at[b, c, j], xd_s.at[b, j, c],
            xd_r.at[b, j, c], to_tp(j),
        )

    def xb_copy(b, j, c):
        return remote(
            res.at[b, c, j], back.at[b, c, t], xb_s.at[b, j, c],
            xb_r.at[b, t, c], to_tp(j),
        )

    def xb_from(b, j, c):
        return remote(
            res.at[b, c, j], back.at[b, c, j], xb_s.at[b, j, c],
            xb_r.at[b, j, c], to_tp(j),
        )

    def rs_copy(b, c, side):
        return remote(
            part.at[b, c], (rin_r if side == 0 else rin_l).at[b, c],
            rs_s.at[b, c], (rs_r if side == 0 else rs_l).at[b, c],
            to_ep(left if side == 0 else right),
        )

    def rs_send(b, c):
        @pl.when(b > z)
        def _():
            rs_copy(b, c, 1).start()

        @pl.when(b < z)
        def _():
            rs_copy(b, c, 0).start()

    expert_row = lax.broadcasted_iota(jnp.int32, (experts, tokens), 0)
    named = [(expert_row == ids[k : k + 1, :]).astype(jnp.float32) for k in range(choose)]
    total = named[0]
    for k in range(1, choose):
        total = total + named[k]
    before = (
        lax.broadcasted_iota(jnp.int32, (tokens, tokens), 0)
        < lax.broadcasted_iota(jnp.int32, (tokens, tokens), 1)
    ).astype(jnp.bfloat16)
    counts = jnp.dot(total.astype(jnp.bfloat16), before, preferred_element_type=jnp.float32)
    first = expert_row.astype(jnp.float32) * cap + counts
    lines = [jnp.sum(named[k] * first, axis=0, keepdims=True) for k in range(choose)]
    lines += [wts[k : k + 1, :] for k in range(choose)]
    lines.append(jnp.zeros((meta.shape[1] - 2 * choose, tokens), jnp.float32))
    meta[z] = jnp.concatenate(lines, axis=0)

    hidden = hid[...].astype(jnp.float32)
    scale = lax.rsqrt(jnp.mean(hidden * hidden, axis=-1, keepdims=True) + 1e-06)
    for c in range(chunks):
        normed = hidden[:, c * cw : (c + 1) * cw] * scale * gain[:, cols(c)]
        ag[z, c] = normed.astype(jnp.bfloat16)

    partners = (m - 1) + (z > 0).astype(jnp.int32) + (z < n - 1).astype(jnp.int32)
    pl.semaphore_wait(barrier, partners)

    @pl.when(z > 0)
    def _():
        me_copy(z, 0).start()

    @pl.when(z < n - 1)
    def _():
        me_copy(z, 1).start()

    for c in range(chunks):
        @pl.when(z > 0)
        def _(c=c):
            ag_copy(z, c, 0).start()

        @pl.when(z < n - 1)
        def _(c=c):
            ag_copy(z, c, 1).start()

    def receive(b, c):
        if c == 0:
            me_copy(b, 0).wait_recv()
        ag_copy(b, c, 0).wait_recv()

    def forward(s):
        b = order[s]
        for c in range(chunks):
            receive(b, c)

            @pl.when(b < z)
            def _(c=c):
                if c == 0:
                    me_copy(b, 1).start()
                ag_copy(b, c, 1).start()

            @pl.when(b > z)
            def _(c=c):
                if c == 0:
                    me_copy(b, 0).start()
                ag_copy(b, c, 0).start()

    def slot_row():
        row = lax.broadcasted_iota(jnp.int32, (rows, tokens), 0) + z * rows
        return row.astype(jnp.float32)

    def dispatch(s, wait):
        b = order[s]
        select = None
        for c in range(chunks):
            if wait:
                receive(b, c)
            if select is None:
                info = meta[b]
                row = slot_row()
                select = jnp.zeros((rows, tokens), jnp.float32)
                for k in range(choose):
                    select = select + (row == info[k : k + 1, :]).astype(jnp.float32)
                select = select.astype(jnp.bfloat16)
            sent = jnp.dot(select, ag[b, c], preferred_element_type=jnp.float32)
            q = c // ratio
            inner = pl.ds((c % ratio) * cw, cw)
            disp[b, q, :, :, inner] = sent.astype(jnp.bfloat16).reshape(m, cap, cw)
            if (c + 1) % ratio == 0:
                for d in range(m - 1, 0, -1):
                    xd_copy(b, lax.rem(t + d, m), q).start()
                xin[b, q, t] = disp[b, q, t]

    def experts_step(s):
        b = order[s]
        if s == 0:
            loads[0].wait()
            loads[1].wait()
        gate_act = jnp.zeros((rows, gate.shape[1]), jnp.float32)
        up_act = jnp.zeros((rows, gate.shape[1]), jnp.float32)
        for q in range(xchunks):
            for d in range(1, m):
                xd_from(b, lax.rem(t + d, m), q).wait_recv()
            block = xin[b, q].reshape(rows, xw)
            gate_act += jnp.dot(block, gate[xcols(q), :], preferred_element_type=jnp.float32)
            up_act += jnp.dot(block, up[xcols(q), :], preferred_element_type=jnp.float32)
        act = (gate_act / (1.0 + jnp.exp(-gate_act)) * up_act).astype(jnp.bfloat16)
        if s == 0:
            loads[2].wait()
        for q in range(xchunks):
            made = jnp.dot(act, down[:, xcols(q)], preferred_element_type=jnp.float32)
            res[b, q] = made.astype(jnp.bfloat16).reshape(m, cap, xw)
            for d in range(m - 1, 0, -1):
                xb_copy(b, lax.rem(t + d, m), q).start()
            back[b, q, t] = res[b, q, t]

    def combine(s):
        b = order[s]
        info = meta[b]
        row = slot_row()
        mix = jnp.zeros((rows, tokens), jnp.float32)
        for k in range(choose):
            mix = mix + jnp.where(
                row == info[k : k + 1, :], info[choose + k : choose + k + 1, :], 0.0
            )
        mix = jnp.transpose(mix).astype(jnp.bfloat16)
        for c in range(chunks):
            q = c // ratio
            if c % ratio == 0:
                for d in range(1, m):
                    xb_from(b, lax.rem(t + d, m), q).wait_recv()
            block = back[b, q, :, :, pl.ds((c % ratio) * cw, cw)].reshape(rows, cw)
            value = jnp.dot(mix, block, preferred_element_type=jnp.float32)
            if s == 0:
                acc[:, cols(c)] = value
            else:
                part[b, c] = value.astype(jnp.bfloat16)

                @pl.when(end)
                def _(c=c, b=b):
                    rs_send(b, c)

    dispatch(0, False)
    experts_step(0)

    @pl.when(end)
    def _():
        for s in range(1, n):
            dispatch(s, True)
            if s == 1:
                combine(0)
            experts_step(s)
            combine(s)

    @pl.when(middle)
    def _():
        forward(1)
        forward(2)
        dispatch(1, False)
        dispatch(2, False)
        combine(0)
        for s in range(1, n):
            experts_step(s)
            if s + 2 < n:
                forward(s + 2)
                dispatch(s + 2, False)
            if s > 1:
                combine(s - 1)
        combine(n - 1)

    def due(q):
        return sorted(
            [b for b in range(n) if b != q],
            key=lambda b: (b, q) if b > q else (n - 1 - b, n - 1 - q),
        )

    dues = [due(q) for q in range(n)]
    later = [pick(z, [dues[q][s] for q in range(n)]) for s in range(n - 1)]

    @pl.when(middle)
    def _():
        def add(b, c):
            @pl.when(b > z)
            def _():
                rs_copy(b, c, 1).wait_recv()
                part[b, c] = part[b, c] + rin_l[b, c]

            @pl.when(b < z)
            def _():
                rs_copy(b, c, 0).wait_recv()
                part[b, c] = part[b, c] + rin_r[b, c]

            rs_send(b, c)

        for b in later[:-2]:
            for c in range(chunks):
                add(b, c)
        for c in range(chunks):
            for b in later[-2:]:
                add(b, c)

    for c in range(chunks):
        @pl.when(z > 0)
        def _(c=c):
            rs_copy(z, c, 1).wait_recv()
            acc[:, cols(c)] = acc[:, cols(c)] + rin_l[z, c].astype(jnp.float32)

        @pl.when(z < n - 1)
        def _(c=c):
            rs_copy(z, c, 0).wait_recv()
            acc[:, cols(c)] = acc[:, cols(c)] + rin_r[z, c].astype(jnp.float32)

        out[:, cols(c)] = acc[:, cols(c)].astype(jnp.bfloat16)

    for s in range(n):
        b = order[s]

        @pl.when(jnp.logical_and(b >= z, z > 0))
        def _(b=b):
            me_copy(b, 0).wait_send()
            for c in range(chunks):
                ag_copy(b, c, 0).wait_send()

        @pl.when(jnp.logical_and(b <= z, z < n - 1))
        def _(b=b):
            me_copy(b, 1).wait_send()
            for c in range(chunks):
                ag_copy(b, c, 1).wait_send()

        for c in range(chunks):
            if s > 0:
                rs_copy(b, c, 0).wait_send()
        for q in range(xchunks):
            for d in range(1, m):
                xd_copy(b, lax.rem(t + d, m), q).wait_send()
                xb_copy(b, lax.rem(t + d, m), q).wait_send()


def fused(n, m, cap, hidden_in, expert_ids, route_weights, norm_gain, gate_proj, up_proj, down_proj):
    tokens, width = hidden_in.shape
    units = gate_proj.shape[2]
    chunks, xchunks = Z_CHUNKS, X_CHUNKS
    cw, xw = width // chunks, width // xchunks
    choose = expert_ids.shape[1]
    lines = -(-2 * choose // 8) * 8
    bf = jnp.bfloat16
    dma = pltpu.SemaphoreType.DMA
    vmem = pl.BlockSpec(memory_space=pltpu.VMEM)
    hbm = pl.BlockSpec(memory_space=pl.ANY)
    return pl.pallas_call(
        functools.partial(kernel, n, m, cap, chunks, xchunks),
        out_shape=jax.ShapeDtypeStruct((tokens, width), bf),
        in_specs=[vmem] * 4 + [hbm] * 3,
        out_specs=vmem,
        scratch_shapes=[
            pltpu.VMEM((n, chunks, tokens, cw), bf),
            pltpu.VMEM((n, lines, tokens), jnp.float32),
            pltpu.VMEM((n, xchunks, m, cap, xw), bf),
            pltpu.VMEM((n, xchunks, m, cap, xw), bf),
            pltpu.VMEM((n, xchunks, m, cap, xw), bf),
            pltpu.VMEM((n, xchunks, m, cap, xw), bf),
            pltpu.VMEM((n, chunks, tokens, cw), bf),
            pltpu.VMEM((n, chunks, tokens, cw), bf),
            pltpu.VMEM((n, chunks, tokens, cw), bf),
            pltpu.VMEM((tokens, width), jnp.float32),
            pltpu.VMEM((width, units), bf),
            pltpu.VMEM((width, units), bf),
            pltpu.VMEM((units, width), bf),
            dma((3,)),
            dma((2, n, chunks)), dma((n, chunks)),
            dma((2, n)), dma((n,)),
            dma((n, m, xchunks)), dma((n, m, xchunks)),
            dma((n, m, xchunks)), dma((n, m, xchunks)),
            dma((n, chunks)), dma((n, chunks)), dma((n, chunks)),
        ],
        compiler_params=pltpu.CompilerParams(
            collective_id=0, has_side_effects=True, vmem_limit_bytes=48 * 1024 * 1024
        ),
        name="experts",
    )(
        hidden_in, expert_ids.T, route_weights.T, norm_gain.reshape(1, -1),
        gate_proj, up_proj, down_proj,
    )


def by_slots(capacity, hidden_in, expert_ids, route_weights, norm_gain, gate_proj, up_proj, down_proj):
    token_count = hidden_in.shape[0]
    model_width = hidden_in.shape[1]
    choose_count = expert_ids.shape[1]
    expert_count = lax.axis_size("ep") * lax.axis_size("tp")
    as_float = hidden_in.astype(jnp.float32)
    scaled = as_float * lax.rsqrt(jnp.mean(as_float * as_float, axis=-1, keepdims=True) + 1e-06)
    normed = (scaled * norm_gain).astype(jnp.bfloat16)
    flat_ids = expert_ids.reshape(-1)
    onehot = (flat_ids[:, None] == jnp.arange(expert_count, dtype=jnp.int32)[None, :]).astype(
        jnp.int32
    )
    slot_index = jnp.sum((jnp.cumsum(onehot, axis=0) - onehot) * onehot, axis=1)
    target = flat_ids * capacity + slot_index
    routed = jnp.repeat(normed, choose_count, axis=0)
    buffer = jnp.zeros((expert_count * capacity, model_width), jnp.bfloat16).at[target].set(routed)
    buffer = buffer.reshape(expert_count, capacity, model_width)
    arrived = lax.all_to_all(buffer, ("ep", "tp"), split_axis=0, concat_axis=0, tiled=True)
    shape_in = arrived.shape
    block_in = arrived.reshape(-1, model_width)
    gate_act = jnp.dot(block_in, gate_proj[0], preferred_element_type=jnp.float32)
    up_act = jnp.dot(block_in, up_proj[0], preferred_element_type=jnp.float32)
    hidden = (jax.nn.silu(gate_act) * up_act).astype(jnp.bfloat16)
    result = jnp.dot(hidden, down_proj[0], preferred_element_type=jnp.float32).astype(jnp.bfloat16)
    results = result.reshape(shape_in)
    returned = lax.all_to_all(results, ("ep", "tp"), split_axis=0, concat_axis=0, tiled=True)
    picked = returned.reshape(-1, model_width)[target].astype(jnp.float32)
    picked = picked.reshape(token_count, choose_count, model_width)
    return jnp.sum(picked * route_weights[:, :, None], axis=1).astype(jnp.bfloat16)


def body(hidden_in, expert_ids, *rest):
    n, m = lax.axis_size("ep"), lax.axis_size("tp")
    tokens = hidden_in.shape[0]
    cap = slot_capacity(expert_ids.shape[1], tokens, n * m)
    if n > 2 and m * cap >= tokens and cap % 16 == 0:
        return fused(n, m, cap, hidden_in, expert_ids, *rest)
    return by_slots(cap, hidden_in, expert_ids, *rest)


def solution(mesh):
    return jax.shard_map(
        body,
        mesh=mesh,
        in_specs=(
            P(("grp", "ep", "tp"), None),
            P(("grp", "ep", "tp"), None),
            P(("grp", "ep", "tp"), None),
            P(),
            P(("ep", "tp"), None, None),
            P(("ep", "tp"), None, None),
            P(("ep", "tp"), None, None),
        ),
        out_specs=P(("grp", "ep", "tp"), None),
        check_vma=False,
    )
```

profile of v0, /device:TPU:0, one launch (start us, length us, event | category | flops | bytes accessed | tf_op | source)
XLA Modules:
  0.0 95.4 jit_solution(16868800398922988526)
XLA Ops:
  0.0 0.0 copy-start
  0.0 1.6 %copy-done = bf16[1,2048,512]{2,1,0:T(8,128)(2,1)S(1)} copy-done((bf16[1,2048,512]{2,1,0:T(8,128)(2,1)S(1)}, bf16[1,2048,512]{2,1,0:T(8,128)(2,1)}, u32[]{:S(2)}) %copy-start) | copy-done | bytes 2097176
  1.6 0.0 copy-start.1
  1.6 1.6 %copy-done.1 = bf16[1,2048,512]{2,1,0:T(8,128)(2,1)S(1)} copy-done((bf16[1,2048,512]{2,1,0:T(8,128)(2,1)S(1)}, bf16[1,2048,512]{2,1,0:T(8,128)(2,1)}, u32[]{:S(2)}) %copy-start.1) | copy-done | bytes 2097176
  3.2 0.0 copy-start.2
  3.2 1.0 %copy-done.2 = bf16[128,2048]{1,0:T(8,128)(2,1)S(1)} copy-done((bf16[128,2048]{1,0:T(8,128)(2,1)S(1)}, bf16[128,2048]{1,0:T(8,128)(2,1)}, u32[]{:S(2)}) %copy-start.2) | copy-done | bytes 524312
  4.2 0.0 copy-start.3
  4.2 0.7 copy-done.3
  4.9 0.0 copy-start.4
  4.9 0.7 copy-done.4
  5.6 0.0 copy-start.5
  5.6 0.7 copy-done.5
  6.3 88.3 %experts.1 = bf16[128,2048]{1,0:T(8,128)(2,1)S(1)} custom-call(bf16[128,2048]{1,0:T(8,128)(2,1)S(1)} %copy-done.2, s32[2,128]{1,0:T(2,128)S(1)} %bitcast.4, f32[2,128]{1,0:T(2,128)S(1)} %bitcast.5, f32[1,2048]{1,0:T(1,128)S(1)} %bitcast.3, bf16[1,2048,512]{2,1,0:T(8,128)(2,1)S(1)} %copy-done, bf16[1,2048,512]{2,1,0:T(8,128)(2,1)S(1)} %copy-done.1, ...), custom_call_target="tpu_custom_call" | custom-call | tf_op jit(solution)/shard_map/experts/pallas_call | solution.py:389
  94.6 0.8 copy.9
Async XLA Ops:
  0.0 1.6 %copy-start = (bf16[1,2048,512]{2,1,0:T(8,128)(2,1)S(1)}, bf16[1,2048,512]{2,1,0:T(8,128)(2,1)}, u32[]{:S(2)}) copy-start(bf16[1,2048,512]{2,1,0:T(8,128)(2,1)} %gate_hbm.1) | copy-start | bytes 6291460
  1.6 1.6 %copy-start.1 = (bf16[1,2048,512]{2,1,0:T(8,128)(2,1)S(1)}, bf16[1,2048,512]{2,1,0:T(8,128)(2,1)}, u32[]{:S(2)}) copy-start(bf16[1,2048,512]{2,1,0:T(8,128)(2,1)} %up_hbm.1) | copy-start | bytes 6291460
  3.2 1.0 %copy-start.2 = (bf16[128,2048]{1,0:T(8,128)(2,1)S(1)}, bf16[128,2048]{1,0:T(8,128)(2,1)}, u32[]{:S(2)}) copy-start(bf16[128,2048]{1,0:T(8,128)(2,1)} %hid.1) | copy-start | bytes 1572868
  4.2 0.7 copy-start.3
  4.9 0.7 copy-start.4
  5.6 0.7 copy-start.5
where the time goes:
time: 95.7 us; the launch traced here: 95.4 us
  Pallas kernels  88.3 us (92%)
  local copies, waits for them, and re-layouts  7.07 us (7%)
    pallas_call x1, Pallas kernels, fused(): pl.pallas_call(functools.partial(kernel, n, m, cap, chunks, xchunks), out...  88.3 us
    unnamed x13, local copies, waits for them, and re-layouts  7.07 us

commit v1 on v0

v1 whole, which is shorter than its diff:
```python
import functools

import jax
import jax.numpy as jnp
from jax import lax
from jax.experimental import pallas as pl
from jax.experimental.pallas import tpu as pltpu
from jax.sharding import PartitionSpec as P

CHUNKS = 4
OWN, OUTER, INNER, FAR = 0, 1, 2, 3


def slot_capacity(choose_count, token_count, expert_count):
    return max(2, 2 * choose_count * token_count // expert_count)


def kernel(
    n, m, cap, chunks,
    hid_hbm, ids_hbm, wts_hbm, gain_hbm, gate_hbm, up_hbm, down_hbm, out,
    hid, ids, wts, gain, gate, up, down,
    tok, meta, mixes, dsp, dse, xin, res, back, esl, part, rin, acc, pre,
    in_sem, ag_s, ag_r, me_s, me_r, xd_s, xd_r, de_s, xb_s, xb_r, es_s, es_r, rs_s, rs_r,
):
    z = lax.axis_index("ep")
    t = lax.axis_index("tp")
    tokens, width = hid.shape
    rows = m * cap
    cw = width // chunks
    choose = ids.shape[0]
    experts = n * m
    middle = jnp.logical_and(z > 0, z < n - 1)
    end = jnp.logical_or(z == 0, z == n - 1)
    inner = n - 1 - z
    outer = jnp.where(z <= 1, 0, n - 1)
    near = jnp.where(z == 0, 1, n - 2)

    def cols(c):
        return pl.ds(c * cw, cw)

    loads = [
        pltpu.make_async_copy(src, dst, in_sem.at[i])
        for i, (src, dst) in enumerate([
            (hid_hbm, hid), (ids_hbm, ids), (wts_hbm, wts), (gain_hbm, gain),
            (gate_hbm.at[0], gate), (up_hbm.at[0], up), (down_hbm.at[0], down),
        ])
    ]
    for load in loads:
        load.start()

    barrier = pltpu.get_barrier_semaphore()

    def greet(dev):
        pl.semaphore_signal(
            barrier, inc=1, device_id=dev, device_id_type=pl.DeviceIdType.MESH
        )

    for d in range(1, m):
        greet({"tp": lax.rem(t + d, m)})

    @pl.when(middle)
    def _():
        greet({"ep": inner})
        for j in range(m):
            greet({"ep": outer, "tp": jnp.int32(j)})

    @pl.when(end)
    def _():
        for j in range(m):
            greet({"ep": near, "tp": jnp.int32(j)})

    def remote(src, dst, s_sem, r_sem, dev):
        return pltpu.make_async_remote_copy(
            src_ref=src, dst_ref=dst, send_sem=s_sem, recv_sem=r_sem,
            device_id=dev, device_id_type=pl.DeviceIdType.MESH,
        )

    def ag_copy(src, dst, slot, c, dev):
        return remote(tok.at[src, c], tok.at[dst, c], ag_s.at[slot, c], ag_r.at[dst, c], dev)

    def me_copy(src, dst, slot, dev):
        return remote(meta.at[src], meta.at[dst], me_s.at[slot], me_r.at[dst], dev)

    def xd_copy(r, j, c):
        return remote(
            dsp.at[r, c, j], xin.at[r, c, t], xd_s.at[r, j, c], xd_r.at[r, t, c], {"tp": j}
        )

    def xd_from(r, j, c):
        return remote(
            dsp.at[r, c, j], xin.at[r, c, j], xd_s.at[r, j, c], xd_r.at[r, j, c], {"tp": j}
        )

    def de_copy(i, j, c):
        return remote(
            dse.at[i, c, j], xin.at[i + 1, c, t], de_s.at[i, j, c], xd_r.at[i + 1, t, c],
            {"ep": outer, "tp": jnp.int32(j)},
        )

    def xb_copy(r, j, c):
        return remote(
            res.at[r, c, j], back.at[r, c, t], xb_s.at[r, j, c], xb_r.at[r, t, c], {"tp": j}
        )

    def xb_from(r, j, c):
        return remote(
            res.at[r, c, j], back.at[r, c, j], xb_s.at[r, j, c], xb_r.at[r, j, c], {"tp": j}
        )

    def es_copy(i, c):
        return remote(back.at[i + 1, c], esl.at[i, c], es_s.at[i, c], es_r.at[i, c], {"ep": near})

    def rs_copy(i, k, c, dev):
        return remote(part.at[i, c], rin.at[k, c], rs_s.at[i, c], rs_r.at[k, c], dev)

    def peers():
        return [lax.rem(t + d, m) for d in range(m - 1, 0, -1)]

    loads[1].wait()
    loads[2].wait()
    expert_row = lax.broadcasted_iota(jnp.int32, (experts, tokens), 0)
    named = [(expert_row == ids[k : k + 1, :]).astype(jnp.float32) for k in range(choose)]
    total = named[0]
    for k in range(1, choose):
        total = total + named[k]
    before = (
        lax.broadcasted_iota(jnp.int32, (tokens, tokens), 0)
        < lax.broadcasted_iota(jnp.int32, (tokens, tokens), 1)
    ).astype(jnp.bfloat16)
    counts = jnp.dot(total.astype(jnp.bfloat16), before, preferred_element_type=jnp.float32)
    first = expert_row.astype(jnp.float32) * cap + counts
    lines = [jnp.sum(named[k] * first, axis=0, keepdims=True) for k in range(choose)]
    lines += [wts[k : k + 1, :] for k in range(choose)]
    lines.append(jnp.zeros((meta.shape[1] - 2 * choose, tokens), jnp.float32))
    meta[OWN] = jnp.concatenate(lines, axis=0)

    loads[0].wait()
    loads[3].wait()
    hidden = hid[...].astype(jnp.float32)
    scale = lax.rsqrt(jnp.mean(hidden * hidden, axis=-1, keepdims=True) + 1e-06)
    for c in range(chunks):
        normed = hidden[:, c * cw : (c + 1) * cw] * scale * gain[:, cols(c)]
        tok[OWN, c] = normed.astype(jnp.bfloat16)

    def slot_rows(sides):
        parts = [
            lax.broadcasted_iota(jnp.int32, (rows, tokens), 0) + side * rows for side in sides
        ]
        return jnp.concatenate(parts, axis=0).astype(jnp.float32)

    def selection(r, sides):
        info = meta[r]
        row = slot_rows(sides)
        select = jnp.zeros(row.shape, jnp.float32)
        for k in range(choose):
            select = select + (row == info[k : k + 1, :]).astype(jnp.float32)
        return select.astype(jnp.bfloat16)

    def mixing(r, sides):
        info = meta[r]
        row = slot_rows(sides)
        mix = jnp.zeros(row.shape, jnp.float32)
        for k in range(choose):
            mix = mix + jnp.where(
                row == info[k : k + 1, :], info[choose + k : choose + k + 1, :], 0.0
            )
        mixes[r, :, 0 : len(sides) * rows] = jnp.transpose(mix).astype(jnp.bfloat16)

    def dispatch(r, c, select, split):
        sent = jnp.dot(select, tok[r, c], preferred_element_type=jnp.float32).astype(jnp.bfloat16)
        if split:
            i = 0 if r == OWN else r - 1
            dse[i, c] = sent[rows:, :].reshape(m, cap, cw)
            for j in range(m):
                de_copy(i, j, c).start()
        dsp[r, c] = sent[0:rows, :].reshape(m, cap, cw)
        for j in peers():
            xd_copy(r, j, c).start()
        xin[r, c, t] = dsp[r, c, t]

    def experts_step(r, direct):
        if r == (1 if direct else INNER):
            loads[4].wait()
            loads[5].wait()
        gate_act = jnp.zeros((rows, gate.shape[1]), jnp.float32)
        up_act = jnp.zeros((rows, gate.shape[1]), jnp.float32)
        for c in range(chunks):
            for j in ([jnp.int32(j) for j in range(m)] if direct else peers()):
                xd_from(r, j, c).wait_recv()
            block = xin[r, c].reshape(rows, cw)
            gate_act += jnp.dot(block, gate[cols(c), :], preferred_element_type=jnp.float32)
            up_act += jnp.dot(block, up[cols(c), :], preferred_element_type=jnp.float32)
        act = (gate_act / (1.0 + jnp.exp(-gate_act)) * up_act).astype(jnp.bfloat16)
        if r == (1 if direct else INNER):
            loads[6].wait()
        for c in range(chunks):
            made = jnp.dot(act, down[:, cols(c)], preferred_element_type=jnp.float32)
            res[r, c] = made.astype(jnp.bfloat16).reshape(m, cap, cw)
            for j in peers():
                xb_copy(r, j, c).start()
            back[r, c, t] = res[r, c, t]

    def returned(r, c):
        for j in peers():
            xb_from(r, j, c).wait_recv()

    def combined(r, c, i):
        value = jnp.dot(
            mixes[r, :, 0:rows], back[r, c].reshape(rows, cw), preferred_element_type=jnp.float32
        )
        if i is not None:
            value = value + jnp.dot(
                mixes[r, :, rows : 2 * rows], esl[i, c].reshape(rows, cw),
                preferred_element_type=jnp.float32,
            )
        return value

    @pl.when(middle)
    def _():
        pl.semaphore_wait(barrier, 2 * m)
        to_in, to_out = {"ep": inner}, {"ep": outer}
        me_copy(OWN, INNER, 0, to_in).start()
        for c in range(chunks):
            ag_copy(OWN, INNER, 0, c, to_in).start()
        sides = [z, outer]
        select = selection(OWN, sides)
        for c in range(chunks):
            dispatch(OWN, c, select, True)
        mixing(OWN, sides)

        sel_o = sel_i = None
        for c in range(chunks):
            if c == 0:
                me_copy(OWN, OUTER, 0, to_in).wait_recv()
                me_copy(OUTER, FAR, 1, to_in).start()
                sel_o = selection(OUTER, [z])
            ag_copy(OWN, OUTER, 0, c, to_in).wait_recv()
            ag_copy(OUTER, FAR, 1, c, to_in).start()
            if c == 0:
                me_copy(OWN, INNER, 0, to_in).wait_recv()
                sel_i = selection(INNER, sides)
            ag_copy(OWN, INNER, 0, c, to_in).wait_recv()
            dispatch(INNER, c, sel_i, True)
            dispatch(OUTER, c, sel_o, False)
        mixing(OUTER, [z])
        mixing(INNER, sides)

        me_copy(OUTER, FAR, 1, to_in).wait_recv()
        sel_f = selection(FAR, sides)
        for c in range(chunks):
            ag_copy(OUTER, FAR, 1, c, to_in).wait_recv()
            dispatch(FAR, c, sel_f, True)
            if c == 0:
                experts_step(INNER, False)
        mixing(FAR, sides)
        experts_step(FAR, False)
        experts_step(OUTER, False)
        experts_step(OWN, False)

        def to_inner(i, r, e, c):
            returned(r, c)
            es_copy(e, c).wait_recv()
            part[i, c] = combined(r, c, e).astype(jnp.bfloat16)
            rs_copy(i, i, c, to_in).start()

        def to_outer(c):
            rs_copy(1, 1, c, to_in).wait_recv()
            part[2, c] = (pre[c] + rin[1, c].astype(jnp.float32)).astype(jnp.bfloat16)
            rs_copy(2, 0, c, to_out).start()

        for c in range(chunks):
            to_inner(0, INNER, 1, c)
        for c in range(chunks):
            returned(OUTER, c)
            pre[c] = combined(OUTER, c, None)
        for c in range(chunks):
            returned(OWN, c)
            es_copy(0, c).wait_recv()
            acc[:, cols(c)] = combined(OWN, c, 0)
        lag = 2
        for c in range(chunks + lag):
            if c < chunks:
                to_inner(1, FAR, 2, c)
                rs_copy(0, 0, c, to_in).wait_recv()
                value = acc[:, cols(c)] + rin[0, c].astype(jnp.float32)
                out[:, cols(c)] = value.astype(jnp.bfloat16)
            if c >= lag:
                to_outer(c - lag)

        for s in range(2):
            me_copy(OWN, INNER, s, to_in).wait_send()
            for c in range(chunks):
                ag_copy(OWN, INNER, s, c, to_in).wait_send()
        for c in range(chunks):
            for j in range(m):
                for i in range(3):
                    de_copy(i, j, c).wait_send()
            for r in range(4):
                for j in peers():
                    xd_copy(r, j, c).wait_send()
                    xb_copy(r, j, c).wait_send()
            for i in range(3):
                rs_copy(i, 0, c, to_in).wait_send()

    @pl.when(end)
    def _():
        pl.semaphore_wait(barrier, 2 * m - 1)
        to_near = {"ep": near}
        me_copy(OWN, OUTER, 0, to_near).start()
        for c in range(chunks):
            ag_copy(OWN, OUTER, 0, c, to_near).start()
        select = selection(OWN, [z])
        for c in range(chunks):
            dispatch(OWN, c, select, False)
        mixing(OWN, [z])
        for r in range(1, 4):
            experts_step(r, True)
            for c in range(chunks):
                returned(r, c)
                es_copy(r - 1, c).start()
        experts_step(OWN, False)
        for c in range(chunks):
            returned(OWN, c)
            acc[:, cols(c)] = combined(OWN, c, None)
        for c in range(chunks):
            rs_copy(2, 0, c, to_near).wait_recv()
            value = acc[:, cols(c)] + rin[0, c].astype(jnp.float32)
            out[:, cols(c)] = value.astype(jnp.bfloat16)

        me_copy(OWN, OUTER, 0, to_near).wait_send()
        for c in range(chunks):
            ag_copy(OWN, OUTER, 0, c, to_near).wait_send()
            for j in peers():
                xd_copy(OWN, j, c).wait_send()
                for r in range(4):
                    xb_copy(r, j, c).wait_send()
            for i in range(3):
                es_copy(i, c).wait_send()


def fused(n, m, cap, hidden_in, expert_ids, route_weights, norm_gain, gate_proj, up_proj, down_proj):
    tokens, width = hidden_in.shape
    units = gate_proj.shape[2]
    chunks = CHUNKS
    cw = width // chunks
    choose = expert_ids.shape[1]
    lines = -(-2 * choose // 8) * 8
    bf, f32 = jnp.bfloat16, jnp.float32
    dma = pltpu.SemaphoreType.DMA
    hbm = pl.BlockSpec(memory_space=pl.ANY)
    slots = lambda k: pltpu.VMEM((k, chunks, m, cap, cw), bf)
    block = lambda k: pltpu.VMEM((k, chunks, tokens, cw), bf)
    return pl.pallas_call(
        functools.partial(kernel, n, m, cap, chunks),
        out_shape=jax.ShapeDtypeStruct((tokens, width), bf),
        in_specs=[hbm] * 7,
        out_specs=pl.BlockSpec(memory_space=pltpu.VMEM),
        scratch_shapes=[
            pltpu.VMEM((tokens, width), bf),
            pltpu.VMEM((choose, tokens), jnp.int32),
            pltpu.VMEM((choose, tokens), f32),
            pltpu.VMEM((1, width), f32),
            pltpu.VMEM((width, units), bf),
            pltpu.VMEM((width, units), bf),
            pltpu.VMEM((units, width), bf),
            block(4),
            pltpu.VMEM((4, lines, tokens), f32),
            pltpu.VMEM((4, tokens, 2 * m * cap), bf),
            slots(4), slots(3), slots(4), slots(4), slots(4), slots(3),
            block(3), block(2),
            pltpu.VMEM((tokens, width), f32),
            pltpu.VMEM((chunks, tokens, cw), f32),
            dma((7,)),
            dma((2, chunks)), dma((4, chunks)),
            dma((2,)), dma((4,)),
            dma((4, m, chunks)), dma((4, m, chunks)), dma((3, m, chunks)),
            dma((4, m, chunks)), dma((4, m, chunks)),
            dma((3, chunks)), dma((3, chunks)),
            dma((3, chunks)), dma((2, chunks)),
        ],
        compiler_params=pltpu.CompilerParams(
            collective_id=0, has_side_effects=True, vmem_limit_bytes=60 * 1024 * 1024
        ),
        name="experts",
    )(
        hidden_in, expert_ids.T, route_weights.T, norm_gain.reshape(1, -1),
        gate_proj, up_proj, down_proj,
    )


def by_slots(capacity, hidden_in, expert_ids, route_weights, norm_gain, gate_proj, up_proj, down_proj):
    token_count = hidden_in.shape[0]
    model_width = hidden_in.shape[1]
    choose_count = expert_ids.shape[1]
    expert_count = lax.axis_size("ep") * lax.axis_size("tp")
    as_float = hidden_in.astype(jnp.float32)
    scaled = as_float * lax.rsqrt(jnp.mean(as_float * as_float, axis=-1, keepdims=True) + 1e-06)
    normed = (scaled * norm_gain).astype(jnp.bfloat16)
    flat_ids = expert_ids.reshape(-1)
    onehot = (flat_ids[:, None] == jnp.arange(expert_count, dtype=jnp.int32)[None, :]).astype(
        jnp.int32
    )
    slot_index = jnp.sum((jnp.cumsum(onehot, axis=0) - onehot) * onehot, axis=1)
    target = flat_ids * capacity + slot_index
    routed = jnp.repeat(normed, choose_count, axis=0)
    buffer = jnp.zeros((expert_count * capacity, model_width), jnp.bfloat16).at[target].set(routed)
    buffer = buffer.reshape(expert_count, capacity, model_width)
    arrived = lax.all_to_all(buffer, ("ep", "tp"), split_axis=0, concat_axis=0, tiled=True)
    shape_in = arrived.shape
    block_in = arrived.reshape(-1, model_width)
    gate_act = jnp.dot(block_in, gate_proj[0], preferred_element_type=jnp.float32)
    up_act = jnp.dot(block_in, up_proj[0], preferred_element_type=jnp.float32)
    hidden = (jax.nn.silu(gate_act) * up_act).astype(jnp.bfloat16)
    result = jnp.dot(hidden, down_proj[0], preferred_element_type=jnp.float32).astype(jnp.bfloat16)
    results = result.reshape(shape_in)
    returned = lax.all_to_all(results, ("ep", "tp"), split_axis=0, concat_axis=0, tiled=True)
    picked = returned.reshape(-1, model_width)[target].astype(jnp.float32)
    picked = picked.reshape(token_count, choose_count, model_width)
    return jnp.sum(picked * route_weights[:, :, None], axis=1).astype(jnp.bfloat16)


def body(hidden_in, expert_ids, *rest):
    n, m = lax.axis_size("ep"), lax.axis_size("tp")
    tokens = hidden_in.shape[0]
    cap = slot_capacity(expert_ids.shape[1], tokens, n * m)
    if n == 4 and m * cap >= tokens and cap % 16 == 0:
        return fused(n, m, cap, hidden_in, expert_ids, *rest)
    return by_slots(cap, hidden_in, expert_ids, *rest)


def solution(mesh):
    return jax.shard_map(
        body,
        mesh=mesh,
        in_specs=(
            P(("grp", "ep", "tp"), None),
            P(("grp", "ep", "tp"), None),
            P(("grp", "ep", "tp"), None),
            P(),
            P(("ep", "tp"), None, None),
            P(("ep", "tp"), None, None),
            P(("ep", "tp"), None, None),
        ),
        out_specs=P(("grp", "ep", "tp"), None),
        check_vma=False,
    )
```

time: 95.7 us -> 79.1 us (0.83)
  Pallas kernels: 88.3 us -> 77 us
  local copies, waits for them, and re-layouts: 7.07 us -> 1.88 us
    pallas_call x1, Pallas kernels: 88.3 us -> 77 us  [fused(): pl.pallas_call(functools.partial(kernel, n, m, cap, chunks), out_shape=ja...]
    unnamed x13 -> x1, local copies, waits for them, and re-layouts: 7.07 us -> 1.88 us
where the time goes in v1:
time: 79.1 us; the launch traced here: 78.9 us
  Pallas kernels  77 us (97%)
  local copies, waits for them, and re-layouts  1.88 us (2%)
    pallas_call x1, Pallas kernels, fused(): pl.pallas_call(functools.partial(kernel, n, m, cap, chunks), out_shape=ja...  77 us
    unnamed x1, local copies, waits for them, and re-layouts  1.88 us

profile of v1, /device:TPU:0, one launch (start us, length us, event | category | flops | bytes accessed | tf_op | source)
XLA Modules:
  0.0 78.9 jit_solution(2906624392569343845)
XLA Ops:
  0.0 77.0 %experts.1 = bf16[128,2048]{1,0:T(8,128)(2,1)} custom-call(bf16[128,2048]{1,0:T(8,128)(2,1)} %hid_hbm.1, s32[2,128]{1,0:T(2,128)} %bitcast.4, f32[2,128]{1,0:T(2,128)} %bitcast.5, f32[1,2048]{1,0:T(1,128)} %bitcast.3, bf16[1,2048,512]{2,1,0:T(8,128)(2,1)} %gate_hbm.1, bf16[1,2048,512]{2,1,0:T(8,128)(2,1)} %up_hbm.1, bf16[1,512,2048]{2,1,0:T(8,128)(2,1)} %down_hbm.1), custom_call_target="tpu_custom_call" | custom-call | tf_op jit(solution)/shard_map/experts/pallas_call | solution.py:353
  77.0 1.9 %copy.9 = bf16[128,2048]{1,0:T(8,128)(2,1)} copy(bf16[128,2048]{1,0:T(8,128)(2,1)} %experts.1) | data formatting | bytes 1048576

commit v2 on v1

v2 whole, which is shorter than its diff:
```python
import functools

import jax
import jax.numpy as jnp
from jax import lax
from jax.experimental import pallas as pl
from jax.experimental.pallas import tpu as pltpu
from jax.sharding import PartitionSpec as P

CHUNKS = 4
BACK_CHUNKS = 8
OWN, OUTER, INNER, FAR = 0, 1, 2, 3


def slot_capacity(choose_count, token_count, expert_count):
    return max(2, 2 * choose_count * token_count // expert_count)


def kernel(
    n, m, cap, chunks, bchunks,
    hid_hbm, ids_hbm, wts_hbm, gain_hbm, gate_hbm, up_hbm, down_hbm, out,
    hid, ids, wts, gain, gate, up, down,
    tok, meta, mixes, dsp, dse, xin, res, back, esl, part, rin, pre,
    in_sem, ag_s, ag_r, me_s, me_r, xd_s, xd_r, de_s, xb_s, xb_r, es_s, es_r, rs_s, rs_r,
):
    z = lax.axis_index("ep")
    t = lax.axis_index("tp")
    tokens, width = hid.shape
    rows = m * cap
    cw = width // chunks
    bw = width // bchunks
    half = cap // 2
    choose = ids.shape[0]
    experts = n * m
    middle = jnp.logical_and(z > 0, z < n - 1)
    end = jnp.logical_or(z == 0, z == n - 1)
    inner = n - 1 - z
    outer = jnp.where(z <= 1, 0, n - 1)
    near = jnp.where(z == 0, 1, n - 2)

    def cols(c):
        return pl.ds(c * cw, cw)

    def bcols(c):
        return pl.ds(c * bw, bw)

    loads = [
        pltpu.make_async_copy(src, dst, in_sem.at[i])
        for i, (src, dst) in enumerate([
            (hid_hbm, hid), (ids_hbm, ids), (wts_hbm, wts), (gain_hbm, gain),
            (gate_hbm.at[0], gate), (up_hbm.at[0], up), (down_hbm.at[0], down),
        ])
    ]
    for load in loads:
        load.start()

    barrier = pltpu.get_barrier_semaphore()

    def greet(dev):
        pl.semaphore_signal(
            barrier, inc=1, device_id=dev, device_id_type=pl.DeviceIdType.MESH
        )

    for d in range(1, m):
        greet({"tp": lax.rem(t + d, m)})

    @pl.when(middle)
    def _():
        greet({"ep": inner})
        for j in range(m):
            greet({"ep": outer, "tp": jnp.int32(j)})

    @pl.when(end)
    def _():
        for j in range(m):
            greet({"ep": near, "tp": jnp.int32(j)})

    def remote(src, dst, s_sem, r_sem, dev):
        return pltpu.make_async_remote_copy(
            src_ref=src, dst_ref=dst, send_sem=s_sem, recv_sem=r_sem,
            device_id=dev, device_id_type=pl.DeviceIdType.MESH,
        )

    def lot(r):
        return r, r, 0, cap

    first_half, second_half = (1, 1, 0, half), (4, 1, half, cap - half)
    others, self_id = pl.ds(0, m - 1), {"tp": t}

    def ag_copy(src, dst, slot, c, dev):
        return remote(tok.at[src, c], tok.at[dst, c], ag_s.at[slot], ag_r.at[dst, c], dev)

    def ag_sent(slot):
        remote(tok.at[0], tok.at[0], ag_s.at[slot], ag_r.at[0, 0], self_id).wait_send()

    def me_copy(src, dst, slot, dev):
        return remote(meta.at[src], meta.at[dst], me_s.at[slot], me_r.at[dst], dev)

    def xd_copy(r, j, c):
        return remote(
            dsp.at[r, c, j], xin.at[r, c, t], xd_s.at[r], xd_r.at[r, c], {"tp": j}
        )

    def xd_from(r, c):
        return remote(
            dsp.at[r, c, others], xin.at[r, c, others], xd_s.at[r], xd_r.at[r, c], self_id
        )

    def xd_sent(r):
        remote(
            dsp.at[r, :, others], xin.at[r, :, others], xd_s.at[r], xd_r.at[r, 0], self_id
        ).wait_send()

    def spread():
        return [lax.rem(t + lax.rem(t, 2) + d, m) for d in range(m)]

    def de_copy(part_of, j, c):
        k, r, lo, size = part_of
        here = pl.ds(lo, size)
        return remote(
            dse.at[r - 1, c, j, here], xin.at[r, c, t, here], de_s.at[k - 1],
            xd_r.at[k, c], {"ep": outer, "tp": j},
        )

    def de_from(part_of, c):
        k, r, lo, size = part_of
        here = pl.ds(lo, size)
        return remote(
            dse.at[r - 1, c, :, here], xin.at[r, c, :, here], de_s.at[k - 1],
            xd_r.at[k, c], self_id,
        )

    def de_sent(part_of):
        k, r, lo, size = part_of
        here = pl.ds(lo, size)
        remote(
            dse.at[r - 1, :, :, here], xin.at[r, :, :, here], de_s.at[k - 1],
            xd_r.at[k, 0], self_id,
        ).wait_send()

    def xb_copy(part_of, j, c):
        k, r, lo, size = part_of
        here = pl.ds(lo, size)
        return remote(
            res.at[r, c, j, here], back.at[r, c, t, here], xb_s.at[k],
            xb_r.at[k, c], {"tp": j},
        )

    def xb_from(part_of, c):
        k, r, lo, size = part_of
        here = pl.ds(lo, size)
        return remote(
            res.at[r, c, others, here], back.at[r, c, others, here], xb_s.at[k],
            xb_r.at[k, c], self_id,
        )

    def xb_sent(part_of):
        k, r, lo, size = part_of
        here = pl.ds(lo, size)
        remote(
            res.at[r, :, others, here], back.at[r, :, others, here], xb_s.at[k],
            xb_r.at[k, 0], self_id,
        ).wait_send()

    def es_copy(part_of, c):
        k, r, lo, size = part_of
        here = pl.ds(lo, size)
        return remote(
            back.at[r, c, :, here], esl.at[r - 1, c, :, here], es_s.at[k - 1],
            es_r.at[k - 1, c], {"ep": near},
        )

    def es_sent(part_of):
        k, r, lo, size = part_of
        here = pl.ds(lo, size)
        remote(
            back.at[r, :, :, here], esl.at[r - 1, :, :, here], es_s.at[k - 1],
            es_r.at[k - 1, 0], self_id,
        ).wait_send()

    def rs_copy(i, k, c, dev):
        return remote(part.at[i, c], rin.at[k, c], rs_s.at[i], rs_r.at[k, c], dev)

    def rs_sent(i):
        remote(part.at[i], rin.at[0], rs_s.at[i], rs_r.at[0, 0], self_id).wait_send()

    def peers():
        return [lax.rem(t + d, m) for d in range(m - 1, 0, -1)]

    loads[1].wait()
    loads[2].wait()
    expert_row = lax.broadcasted_iota(jnp.int32, (experts, tokens), 0)
    named = [(expert_row == ids[k : k + 1, :]).astype(jnp.float32) for k in range(choose)]
    total = named[0]
    for k in range(1, choose):
        total = total + named[k]
    before = (
        lax.broadcasted_iota(jnp.int32, (tokens, tokens), 0)
        < lax.broadcasted_iota(jnp.int32, (tokens, tokens), 1)
    ).astype(jnp.bfloat16)
    counts = jnp.dot(total.astype(jnp.bfloat16), before, preferred_element_type=jnp.float32)
    first = expert_row.astype(jnp.float32) * cap + counts
    lines = [jnp.sum(named[k] * first, axis=0, keepdims=True) for k in range(choose)]
    lines += [wts[k : k + 1, :] for k in range(choose)]
    lines.append(jnp.zeros((meta.shape[1] - 2 * choose, tokens), jnp.float32))
    meta[OWN] = jnp.concatenate(lines, axis=0)

    loads[0].wait()
    loads[3].wait()
    hidden = hid[...].astype(jnp.float32)
    scale = lax.rsqrt(jnp.mean(hidden * hidden, axis=-1, keepdims=True) + 1e-06)
    for c in range(chunks):
        normed = hidden[:, c * cw : (c + 1) * cw] * scale * gain[:, cols(c)]
        tok[OWN, c] = normed.astype(jnp.bfloat16)

    def slot_rows(sides):
        parts = [
            lax.broadcasted_iota(jnp.int32, (rows, tokens), 0) + side * rows for side in sides
        ]
        return jnp.concatenate(parts, axis=0).astype(jnp.float32)

    def selection(r, sides):
        info = meta[r]
        row = slot_rows(sides)
        select = jnp.zeros(row.shape, jnp.float32)
        for k in range(choose):
            select = select + (row == info[k : k + 1, :]).astype(jnp.float32)
        return select.astype(jnp.bfloat16)

    def mixing(r, sides):
        info = meta[r]
        row = slot_rows(sides)
        mix = jnp.zeros(row.shape, jnp.float32)
        for k in range(choose):
            mix = mix + jnp.where(
                row == info[k : k + 1, :], info[choose + k : choose + k + 1, :], 0.0
            )
        mixes[r, :, 0 : len(sides) * rows] = jnp.transpose(mix).astype(jnp.bfloat16)

    def dispatch(r, c, select):
        sent = jnp.dot(select, tok[r, c], preferred_element_type=jnp.float32).astype(jnp.bfloat16)
        if select.shape[0] > rows:
            i = 0 if r == OWN else r - 1
            dse[i, c] = sent[rows:, :].reshape(m, cap, cw)
            for j in spread():
                de_copy(first_half if r == OWN else lot(r), j, c).start()
        dsp[r, c] = sent[0:rows, :].reshape(m, cap, cw)
        for j in peers():
            xd_copy(r, j, c).start()
        xin[r, c, t] = dsp[r, c, t]

    def experts_step(part_of, direct, opening=False, send=True):
        k, r, lo, size = part_of
        if opening:
            loads[4].wait()
            loads[5].wait()
        gate_act = jnp.zeros((m * size, gate.shape[1]), jnp.float32)
        up_act = jnp.zeros((m * size, gate.shape[1]), jnp.float32)
        for c in range(chunks):
            (de_from(part_of, c) if direct else xd_from(r, c)).wait_recv()
            block = xin[r, c, :, lo : lo + size, :].reshape(m * size, cw)
            gate_act += jnp.dot(block, gate[cols(c), :], preferred_element_type=jnp.float32)
            up_act += jnp.dot(block, up[cols(c), :], preferred_element_type=jnp.float32)
        act = (gate_act / (1.0 + jnp.exp(-gate_act)) * up_act).astype(jnp.bfloat16)
        if opening:
            loads[6].wait()
        for c in range(bchunks):
            made = jnp.dot(act, down[:, bcols(c)], preferred_element_type=jnp.float32)
            res[r, c, :, lo : lo + size, :] = made.astype(jnp.bfloat16).reshape(m, size, bw)
            if send:
                send_back(part_of, c)
            back[r, c, t, lo : lo + size, :] = res[r, c, t, lo : lo + size, :]

    def send_back(part_of, c):
        for j in peers():
            xb_copy(part_of, j, c).start()

    def combined(r, c, i):
        value = jnp.dot(
            mixes[r, :, 0:rows], back[r, c].reshape(rows, bw), preferred_element_type=jnp.float32
        )
        if i is not None:
            value = value + jnp.dot(
                mixes[r, :, rows : 2 * rows], esl[i, c].reshape(rows, bw),
                preferred_element_type=jnp.float32,
            )
        return value

    @pl.when(middle)
    def _():
        pl.semaphore_wait(barrier, 2 * m)
        to_in, to_out = {"ep": inner}, {"ep": outer}
        me_copy(OWN, INNER, 0, to_in).start()
        for c in range(chunks):
            ag_copy(OWN, INNER, 0, c, to_in).start()
        sides = [z, outer]
        select = selection(OWN, sides)
        for c in range(chunks):
            dispatch(OWN, c, select)
        mixing(OWN, sides)

        sel_o = sel_i = None
        for c in range(chunks):
            if c == 0:
                me_copy(OWN, INNER, 0, to_in).wait_recv()
                sel_i = selection(INNER, sides)
            ag_copy(OWN, INNER, 0, c, to_in).wait_recv()
            dispatch(INNER, c, sel_i)
            if c == 0:
                me_copy(OWN, OUTER, 0, to_in).wait_recv()
                me_copy(OUTER, FAR, 1, to_in).start()
                sel_o = selection(OUTER, [z])
            ag_copy(OWN, OUTER, 0, c, to_in).wait_recv()
            ag_copy(OUTER, FAR, 1, c, to_in).start()
            dispatch(OUTER, c, sel_o)
        mixing(INNER, sides)
        experts_step(lot(INNER), False, True)

        me_copy(OUTER, FAR, 1, to_in).wait_recv()
        sel_f = selection(FAR, sides)
        for c in range(chunks):
            ag_copy(OUTER, FAR, 1, c, to_in).wait_recv()
            dispatch(FAR, c, sel_f)
        for c in range(chunks):
            for j in spread():
                de_copy(second_half, j, c).start()
        mixing(FAR, sides)
        mixing(OUTER, [z])
        experts_step(lot(OUTER), False, send=False)

        def to_inner(i, r, c):
            xb_from(lot(r), c).wait_recv()
            es_copy(lot(r), c).wait_recv()
            part[i, c] = combined(r, c, r - 1).astype(jnp.bfloat16)
            rs_copy(i, i, c, to_in).start()

        def to_outer(c):
            xb_from(lot(OUTER), c).wait_recv()
            value = combined(OUTER, c, None)
            rs_copy(1, 1, c, to_in).wait_recv()
            part[2, c] = (value + rin[1, c].astype(jnp.float32)).astype(jnp.bfloat16)
            rs_copy(2, 0, c, to_out).start()

        def finish(c):
            xb_from(lot(OWN), c).wait_recv()
            es_copy(first_half, c).wait_recv()
            es_copy(second_half, c).wait_recv()
            rs_copy(0, 0, c, to_in).wait_recv()
            value = combined(OWN, c, 0) + rin[0, c].astype(jnp.float32)
            out[:, bcols(c)] = value.astype(jnp.bfloat16)

        for c in range(bchunks):
            to_inner(0, INNER, c)
            if c == bchunks // 2 - 1:
                experts_step(lot(FAR), False)
                for d in range(bchunks):
                    send_back(lot(OUTER), d)
        experts_step(lot(OWN), False)
        lag = 3
        for c in range(bchunks + lag):
            if c < bchunks:
                to_inner(1, FAR, c)
            if c >= lag:
                to_outer(c - lag)
        for c in range(bchunks):
            finish(c)

        for s in range(2):
            me_copy(OWN, INNER, s, to_in).wait_send()
            ag_sent(s)
        for part_of in (first_half, lot(INNER), lot(FAR), second_half):
            de_sent(part_of)
        for r in range(4):
            xd_sent(r)
            xb_sent(lot(r))
        for i in range(3):
            rs_sent(i)

    @pl.when(end)
    def _():
        pl.semaphore_wait(barrier, 2 * m - 1)
        to_near = {"ep": near}
        me_copy(OWN, OUTER, 0, to_near).start()
        for c in range(chunks):
            ag_copy(OWN, OUTER, 0, c, to_near).start()
        select = selection(OWN, [z])
        early = chunks // 2
        for c in range(early):
            dispatch(OWN, c, select)
        mixing(OWN, [z])
        lots = [first_half, lot(INNER), lot(FAR), second_half]
        for s, part_of in enumerate(lots):
            experts_step(part_of, True, s == 0)
            if s == 0:
                for c in range(early, chunks):
                    dispatch(OWN, c, select)
            for c in range(bchunks):
                xb_from(part_of, c).wait_recv()
                es_copy(part_of, c).start()
        experts_step(lot(OWN), False)
        for c in range(bchunks):
            xb_from(lot(OWN), c).wait_recv()
            pre[c] = combined(OWN, c, None)
        for c in range(bchunks):
            rs_copy(2, 0, c, to_near).wait_recv()
            value = pre[c] + rin[0, c].astype(jnp.float32)
            out[:, bcols(c)] = value.astype(jnp.bfloat16)

        me_copy(OWN, OUTER, 0, to_near).wait_send()
        ag_sent(0)
        xd_sent(OWN)
        xb_sent(lot(OWN))
        for part_of in lots:
            xb_sent(part_of)
            es_sent(part_of)


def fused(n, m, cap, hidden_in, expert_ids, route_weights, norm_gain, gate_proj, up_proj, down_proj):
    tokens, width = hidden_in.shape
    units = gate_proj.shape[2]
    chunks, bchunks = CHUNKS, BACK_CHUNKS
    choose = expert_ids.shape[1]
    lines = -(-2 * choose // 8) * 8
    bf, f32 = jnp.bfloat16, jnp.float32
    dma = pltpu.SemaphoreType.DMA
    hbm = pl.BlockSpec(memory_space=pltpu.HBM)
    slots = lambda k, q: pltpu.VMEM((k, q, m, cap, width // q), bf)
    block = lambda k, q: pltpu.VMEM((k, q, tokens, width // q), bf)
    return pl.pallas_call(
        functools.partial(kernel, n, m, cap, chunks, bchunks),
        out_shape=jax.ShapeDtypeStruct((tokens, width), bf),
        in_specs=[hbm] * 7,
        out_specs=pl.BlockSpec(memory_space=pltpu.VMEM),
        scratch_shapes=[
            pltpu.VMEM((tokens, width), bf),
            pltpu.VMEM((choose, tokens), jnp.int32),
            pltpu.VMEM((choose, tokens), f32),
            pltpu.VMEM((1, width), f32),
            pltpu.VMEM((width, units), bf),
            pltpu.VMEM((width, units), bf),
            pltpu.VMEM((units, width), bf),
            block(4, chunks),
            pltpu.VMEM((4, lines, tokens), f32),
            pltpu.VMEM((4, tokens, 2 * m * cap), bf),
            slots(4, chunks), slots(3, chunks), slots(4, chunks),
            slots(4, bchunks), slots(4, bchunks), slots(3, bchunks),
            block(3, bchunks), block(2, bchunks),
            pltpu.VMEM((bchunks, tokens, width // bchunks), f32),
            dma((7,)),
            dma((2,)), dma((4, chunks)),
            dma((2,)), dma((4,)),
            dma((4,)), dma((5, chunks)), dma((4,)),
            dma((5,)), dma((5, bchunks)),
            dma((4,)), dma((4, bchunks)),
            dma((3,)), dma((2, bchunks)),
        ],
        compiler_params=pltpu.CompilerParams(
            collective_id=0, has_side_effects=True, vmem_limit_bytes=40 * 1024 * 1024
        ),
        name="experts",
    )(*[
        pltpu.with_memory_space_constraint(array, pltpu.HBM)
        for array in (
            hidden_in, expert_ids.T, route_weights.T, norm_gain.reshape(1, -1),
            gate_proj, up_proj, down_proj,
        )
    ])


def by_slots(capacity, hidden_in, expert_ids, route_weights, norm_gain, gate_proj, up_proj, down_proj):
    token_count = hidden_in.shape[0]
    model_width = hidden_in.shape[1]
    choose_count = expert_ids.shape[1]
    expert_count = lax.axis_size("ep") * lax.axis_size("tp")
    as_float = hidden_in.astype(jnp.float32)
    scaled = as_float * lax.rsqrt(jnp.mean(as_float * as_float, axis=-1, keepdims=True) + 1e-06)
    normed = (scaled * norm_gain).astype(jnp.bfloat16)
    flat_ids = expert_ids.reshape(-1)
    onehot = (flat_ids[:, None] == jnp.arange(expert_count, dtype=jnp.int32)[None, :]).astype(
        jnp.int32
    )
    slot_index = jnp.sum((jnp.cumsum(onehot, axis=0) - onehot) * onehot, axis=1)
    target = flat_ids * capacity + slot_index
    routed = jnp.repeat(normed, choose_count, axis=0)
    buffer = jnp.zeros((expert_count * capacity, model_width), jnp.bfloat16).at[target].set(routed)
    buffer = buffer.reshape(expert_count, capacity, model_width)
    arrived = lax.all_to_all(buffer, ("ep", "tp"), split_axis=0, concat_axis=0, tiled=True)
    shape_in = arrived.shape
    block_in = arrived.reshape(-1, model_width)
    gate_act = jnp.dot(block_in, gate_proj[0], preferred_element_type=jnp.float32)
    up_act = jnp.dot(block_in, up_proj[0], preferred_element_type=jnp.float32)
    hidden = (jax.nn.silu(gate_act) * up_act).astype(jnp.bfloat16)
    result = jnp.dot(hidden, down_proj[0], preferred_element_type=jnp.float32).astype(jnp.bfloat16)
    results = result.reshape(shape_in)
    returned = lax.all_to_all(results, ("ep", "tp"), split_axis=0, concat_axis=0, tiled=True)
    picked = returned.reshape(-1, model_width)[target].astype(jnp.float32)
    picked = picked.reshape(token_count, choose_count, model_width)
    return jnp.sum(picked * route_weights[:, :, None], axis=1).astype(jnp.bfloat16)


def body(hidden_in, expert_ids, *rest):
    n, m = lax.axis_size("ep"), lax.axis_size("tp")
    tokens = hidden_in.shape[0]
    cap = slot_capacity(expert_ids.shape[1], tokens, n * m)
    if n == 4 and m * cap >= tokens and cap % 16 == 0:
        return fused(n, m, cap, hidden_in, expert_ids, *rest)
    return by_slots(cap, hidden_in, expert_ids, *rest)


def solution(mesh):
    return jax.shard_map(
        body,
        mesh=mesh,
        in_specs=(
            P(("grp", "ep", "tp"), None),
            P(("grp", "ep", "tp"), None),
            P(("grp", "ep", "tp"), None),
            P(),
            P(("ep", "tp"), None, None),
            P(("ep", "tp"), None, None),
            P(("ep", "tp"), None, None),
        ),
        out_specs=P(("grp", "ep", "tp"), None),
        check_vma=False,
    )
```

time: 79.1 us -> 66.2 us (0.84)
  Pallas kernels: 77 us -> 65.2 us
  local copies, waits for them, and re-layouts: 1.88 us -> 0.8 us
    pallas_call x1, Pallas kernels: 77 us -> 65.2 us  [fused(): pl.pallas_call(functools.partial(kernel, n, m, cap, chunks, bchunks), out...]
    unnamed x1, local copies, waits for them, and re-layouts: 1.88 us -> 0.8 us
where the time goes in v2:
time: 66.2 us; the launch traced here: 66 us
  Pallas kernels  65.2 us (98%)
  local copies, waits for them, and re-layouts  0.8 us (1%)
    pallas_call x1, Pallas kernels, fused(): pl.pallas_call(functools.partial(kernel, n, m, cap, chunks, bchunks), out...  65.2 us

profile of v2, /device:TPU:0, one launch (start us, length us, event | category | flops | bytes accessed | tf_op | source)
XLA Modules:
  0.0 66.0 jit_solution(7656433009294690933)
XLA Ops:
  0.0 65.2 %experts.1 = bf16[128,2048]{1,0:T(8,128)(2,1)S(1)} custom-call(bf16[128,2048]{1,0:T(8,128)(2,1)} %hid_hbm.1, s32[2,128]{1,0:T(2,128)} %bitcast.4, f32[2,128]{1,0:T(2,128)} %bitcast.5, f32[1,2048]{1,0:T(1,128)} %bitcast.3, bf16[1,2048,512]{2,1,0:T(8,128)(2,1)} %gate_hbm.1, bf16[1,2048,512]{2,1,0:T(8,128)(2,1)} %up_hbm.1, bf16[1,512,2048]{2,1,0:T(8,128)(2,1)} %down_hbm.1), custom_call_target="tpu_custom_call" | custom-call | tf_op jit(solution)/shard_map/experts/pallas_call | solution.py:429
  65.2 0.8 %copy.9 = bf16[128,2048]{1,0:T(8,128)(2,1)} copy(bf16[128,2048]{1,0:T(8,128)(2,1)S(1)} %experts.1) | data formatting | bytes 1048576

commit v3 on v2

--- a/solution.py
+++ b/solution.py
@@ -9,6 +9,7 @@
 
 CHUNKS = 4
 BACK_CHUNKS = 8
+STRAIGHT = (0, 2, 2, 0)
 OWN, OUTER, INNER, FAR = 0, 1, 2, 3
 
 
@@ -154,13 +155,21 @@
             xb_r.at[k, c], self_id,
         )
 
-    def xb_sent(part_of):
-        k, r, lo, size = part_of
-        here = pl.ds(lo, size)
+    def xb_sent(part_of, skip=0):
+        k, r, lo, size = part_of
+        here, late = pl.ds(lo, size), pl.ds(skip, bchunks - skip)
         remote(
-            res.at[r, :, others, here], back.at[r, :, others, here], xb_s.at[k],
+            res.at[r, late, others, here], back.at[r, late, others, here], xb_s.at[k],
             xb_r.at[k, 0], self_id,
         ).wait_send()
+
+    def st_copy(part_of, j, c):
+        k, r, lo, size = part_of
+        here = pl.ds(lo, size)
+        return remote(
+            res.at[r, c, j, here], esl.at[r - 1, c, t, here], es_s.at[k - 1],
+            es_r.at[k - 1, c], {"ep": near, "tp": j},
+        )
 
     def es_copy(part_of, c):
         k, r, lo, size = part_of
@@ -249,7 +258,7 @@
             xd_copy(r, j, c).start()
         xin[r, c, t] = dsp[r, c, t]
 
-    def experts_step(part_of, direct, opening=False, send=True):
+    def experts_step(part_of, direct, opening=False, send=True, straight=0):
         k, r, lo, size = part_of
         if opening:
             loads[4].wait()
@@ -267,6 +276,10 @@
         for c in range(bchunks):
             made = jnp.dot(act, down[:, bcols(c)], preferred_element_type=jnp.float32)
             res[r, c, :, lo : lo + size, :] = made.astype(jnp.bfloat16).reshape(m, size, bw)
+            if c < straight:
+                for j in spread():
+                    st_copy(part_of, j, c).start()
+                continue
             if send:
                 send_back(part_of, c)
             back[r, c, t, lo : lo + size, :] = res[r, c, t, lo : lo + size, :]
@@ -314,13 +327,15 @@
             ag_copy(OUTER, FAR, 1, c, to_in).start()
             dispatch(OUTER, c, sel_o)
         mixing(INNER, sides)
-        experts_step(lot(INNER), False, True)
-
         me_copy(OUTER, FAR, 1, to_in).wait_recv()
         sel_f = selection(FAR, sides)
         for c in range(chunks):
             ag_copy(OUTER, FAR, 1, c, to_in).wait_recv()
             dispatch(FAR, c, sel_f)
+            if c == 0:
+                experts_step(lot(INNER), False, True)
+            if c == 1:
+                experts_step(lot(OWN), False, send=False)
         for c in range(chunks):
             for j in spread():
                 de_copy(second_half, j, c).start()
@@ -349,13 +364,18 @@
             value = combined(OWN, c, 0) + rin[0, c].astype(jnp.float32)
             out[:, bcols(c)] = value.astype(jnp.bfloat16)
 
+        ahead = bchunks // 4
         for c in range(bchunks):
             to_inner(0, INNER, c)
-            if c == bchunks // 2 - 1:
+            if c == bchunks // 2:
+                for d in range(ahead):
+                    send_back(lot(OUTER), d)
+            if c == bchunks // 2 + 1:
                 experts_step(lot(FAR), False)
+                for d in range(ahead, bchunks):
+                    send_back(lot(OUTER), d)
                 for d in range(bchunks):
-                    send_back(lot(OUTER), d)
-        experts_step(lot(OWN), False)
+                    send_back(lot(OWN), d)
         lag = 3
         for c in range(bchunks + lag):
             if c < bchunks:
@@ -389,15 +409,30 @@
             dispatch(OWN, c, select)
         mixing(OWN, [z])
         lots = [first_half, lot(INNER), lot(FAR), second_half]
-        for s, part_of in enumerate(lots):
-            experts_step(part_of, True, s == 0)
-            if s == 0:
-                for c in range(early, chunks):
-                    dispatch(OWN, c, select)
-            for c in range(bchunks):
+        relays = [
+            (part_of, c) for k, part_of in enumerate(lots) for c in range(STRAIGHT[k], bchunks)
+        ]
+
+        def relay(until):
+            while relays and relays[0][0][0] in until:
+                part_of, c = relays.pop(0)
                 xb_from(part_of, c).wait_recv()
                 es_copy(part_of, c).start()
+                if part_of[0] == FAR and c == bchunks // 2 - 1:
+                    return
+
+        experts_step(first_half, True, True, straight=STRAIGHT[0])
+        for c in range(early, chunks):
+            dispatch(OWN, c, select)
+        relay((1,))
+        experts_step(lot(INNER), True, straight=STRAIGHT[1])
+        relay((INNER,))
+        experts_step(lot(FAR), True, straight=STRAIGHT[2])
+        relay((FAR,))
+        experts_step(second_half, True, straight=STRAIGHT[3])
+        relay((FAR,))
         experts_step(lot(OWN), False)
+        relay((4,))
         for c in range(bchunks):
             xb_from(lot(OWN), c).wait_recv()
             pre[c] = combined(OWN, c, None)
@@ -410,8 +445,9 @@
         ag_sent(0)
         xd_sent(OWN)
         xb_sent(lot(OWN))
-        for part_of in lots:
-            xb_sent(part_of)
+        for k, part_of in enumerate(lots):
+            if STRAIGHT[k] < bchunks:
+                xb_sent(part_of, STRAIGHT[k])
             es_sent(part_of)
 
 

time: 66.2 us -> 61.8 us (0.934)
  Pallas kernels: 65.2 us -> 60.9 us
    pallas_call x1, Pallas kernels: 65.2 us -> 60.9 us  [fused(): pl.pallas_call(functools.partial(kernel, n, m, cap, chunks, bchunks), out...]
where the time goes in v3:
time: 61.8 us; the launch traced here: 61.7 us
  Pallas kernels  60.9 us (99%)
  local copies, waits for them, and re-layouts  0.8 us (1%)
    pallas_call x1, Pallas kernels, fused(): pl.pallas_call(functools.partial(kernel, n, m, cap, chunks, bchunks), out...  60.9 us

profile of v3, /device:TPU:0, one launch (start us, length us, event | category | flops | bytes accessed | tf_op | source)
XLA Modules:
  0.0 61.7 jit_solution(15673964478339860412)
XLA Ops:
  0.0 60.9 %experts.1 = bf16[128,2048]{1,0:T(8,128)(2,1)S(1)} custom-call(bf16[128,2048]{1,0:T(8,128)(2,1)} %hid_hbm.1, s32[2,128]{1,0:T(2,128)} %bitcast.4, f32[2,128]{1,0:T(2,128)} %bitcast.5, f32[1,2048]{1,0:T(1,128)} %bitcast.3, bf16[1,2048,512]{2,1,0:T(8,128)(2,1)} %gate_hbm.1, bf16[1,2048,512]{2,1,0:T(8,128)(2,1)} %up_hbm.1, bf16[1,512,2048]{2,1,0:T(8,128)(2,1)} %down_hbm.1), custom_call_target="tpu_custom_call" | custom-call | tf_op jit(solution)/shard_map/experts/pallas_call | solution.py:465
  60.9 0.8 %copy.9 = bf16[128,2048]{1,0:T(8,128)(2,1)} copy(bf16[128,2048]{1,0:T(8,128)(2,1)S(1)} %experts.1) | data formatting | bytes 1048576

commit v4 on v3

--- a/solution.py
+++ b/solution.py
@@ -333,12 +333,16 @@
             ag_copy(OUTER, FAR, 1, c, to_in).wait_recv()
             dispatch(FAR, c, sel_f)
             if c == 0:
-                experts_step(lot(INNER), False, True)
+                experts_step(lot(INNER), False, True, send=False)
+                for d in range(4):
+                    send_back(lot(INNER), d)
             if c == 1:
                 experts_step(lot(OWN), False, send=False)
         for c in range(chunks):
             for j in spread():
                 de_copy(second_half, j, c).start()
+        for d in range(4, bchunks):
+            send_back(lot(INNER), d)
         mixing(FAR, sides)
         mixing(OUTER, [z])
         experts_step(lot(OUTER), False, send=False)
@@ -364,24 +368,31 @@
             value = combined(OWN, c, 0) + rin[0, c].astype(jnp.float32)
             out[:, bcols(c)] = value.astype(jnp.bfloat16)
 
-        ahead = bchunks // 4
-        for c in range(bchunks):
-            to_inner(0, INNER, c)
-            if c == bchunks // 2:
+        ahead, soon = bchunks // 4, bchunks * 3 // 8
+        for c in range(soon):
+            if c == soon - 1:
                 for d in range(ahead):
                     send_back(lot(OUTER), d)
-            if c == bchunks // 2 + 1:
-                experts_step(lot(FAR), False)
-                for d in range(ahead, bchunks):
-                    send_back(lot(OUTER), d)
-                for d in range(bchunks):
-                    send_back(lot(OWN), d)
+            to_inner(0, INNER, c)
+        experts_step(lot(FAR), False)
+        for d in range(ahead, bchunks):
+            send_back(lot(OUTER), d)
+        for d in range(bchunks):
+            send_back(lot(OWN), d)
+        late = soon + bchunks * 3 // 8
+        for c in range(soon, late):
+            to_inner(0, INNER, c)
         lag = 3
         for c in range(bchunks + lag):
             if c < bchunks:
                 to_inner(1, FAR, c)
+            elif late < bchunks:
+                to_inner(0, INNER, late)
+                late += 1
             if c >= lag:
                 to_outer(c - lag)
+        for c in range(late, bchunks):
+            to_inner(0, INNER, c)
         for c in range(bchunks):
             finish(c)
 
@@ -409,30 +420,26 @@
             dispatch(OWN, c, select)
         mixing(OWN, [z])
         lots = [first_half, lot(INNER), lot(FAR), second_half]
-        relays = [
-            (part_of, c) for k, part_of in enumerate(lots) for c in range(STRAIGHT[k], bchunks)
-        ]
-
-        def relay(until):
-            while relays and relays[0][0][0] in until:
-                part_of, c = relays.pop(0)
-                xb_from(part_of, c).wait_recv()
-                es_copy(part_of, c).start()
-                if part_of[0] == FAR and c == bchunks // 2 - 1:
-                    return
-
-        experts_step(first_half, True, True, straight=STRAIGHT[0])
+        def relay(k):
+            for c in range(STRAIGHT[k], bchunks):
+                xb_from(lots[k], c).wait_recv()
+                es_copy(lots[k], c).start()
+
+        experts_step(lots[0], True, True, straight=STRAIGHT[0])
         for c in range(early, chunks):
             dispatch(OWN, c, select)
-        relay((1,))
-        experts_step(lot(INNER), True, straight=STRAIGHT[1])
-        relay((INNER,))
-        experts_step(lot(FAR), True, straight=STRAIGHT[2])
-        relay((FAR,))
-        experts_step(second_half, True, straight=STRAIGHT[3])
-        relay((FAR,))
-        experts_step(lot(OWN), False)
-        relay((4,))
+        relay(0)
+        experts_step(lots[1], True, straight=STRAIGHT[1])
+        relay(1)
+        experts_step(lots[2], True, straight=STRAIGHT[2])
+        experts_step(lot(OWN), False, send=False)
+        for c in range(bchunks // 2):
+            send_back(lot(OWN), c)
+        relay(2)
+        experts_step(lots[3], True, straight=STRAIGHT[3])
+        for c in range(bchunks // 2, bchunks):
+            send_back(lot(OWN), c)
+        relay(3)
         for c in range(bchunks):
             xb_from(lot(OWN), c).wait_recv()
             pre[c] = combined(OWN, c, None)

time: 61.8 us -> 61.6 us (level)
  no operation moved by 1% of the time
where the time goes in v4:
time: 61.6 us; the launch traced here: 61.4 us
  Pallas kernels  60.6 us (98%)
  local copies, waits for them, and re-layouts  0.8 us (1%)
    pallas_call x1, Pallas kernels, fused(): pl.pallas_call(functools.partial(kernel, n, m, cap, chunks, bchunks), out...  60.6 us

profile of v4, /device:TPU:0, one launch (start us, length us, event | category | flops | bytes accessed | tf_op | source)
XLA Modules:
  0.0 61.4 jit_solution(9195244196906968939)
XLA Ops:
  0.0 60.6 %experts.1 = bf16[128,2048]{1,0:T(8,128)(2,1)S(1)} custom-call(bf16[128,2048]{1,0:T(8,128)(2,1)} %hid_hbm.1, s32[2,128]{1,0:T(2,128)} %bitcast.4, f32[2,128]{1,0:T(2,128)} %bitcast.5, f32[1,2048]{1,0:T(1,128)} %bitcast.3, bf16[1,2048,512]{2,1,0:T(8,128)(2,1)} %gate_hbm.1, bf16[1,2048,512]{2,1,0:T(8,128)(2,1)} %up_hbm.1, bf16[1,512,2048]{2,1,0:T(8,128)(2,1)} %down_hbm.1), custom_call_target="tpu_custom_call" | custom-call | tf_op jit(solution)/shard_map/experts/pallas_call | solution.py:472
  60.6 0.8 %copy.9 = bf16[128,2048]{1,0:T(8,128)(2,1)} copy(bf16[128,2048]{1,0:T(8,128)(2,1)S(1)} %experts.1) | data formatting | bytes 1048576

commit v5 on v4

--- a/solution.py
+++ b/solution.py
@@ -190,6 +190,13 @@
     def rs_copy(i, k, c, dev):
         return remote(part.at[i, c], rin.at[k, c], rs_s.at[i], rs_r.at[k, c], dev)
 
+    def rs_half(i, k, h, dev):
+        here = pl.ds(h * (tokens // 2), tokens // 2)
+        return remote(
+            part.at[i, bchunks - 1, here], rin.at[k, bchunks - 1, here], rs_s.at[i],
+            rs_r.at[k, bchunks - 1 + h], dev,
+        )
+
     def rs_sent(i):
         remote(part.at[i], rin.at[0], rs_s.at[i], rs_r.at[0, 0], self_id).wait_send()
 
@@ -351,11 +358,23 @@
             xb_from(lot(r), c).wait_recv()
             es_copy(lot(r), c).wait_recv()
             part[i, c] = combined(r, c, r - 1).astype(jnp.bfloat16)
-            rs_copy(i, i, c, to_in).start()
+            if i == 1 and c == bchunks - 1:
+                for h in range(2):
+                    rs_half(1, 1, h, to_in).start()
+            else:
+                rs_copy(i, i, c, to_in).start()
 
         def to_outer(c):
             xb_from(lot(OUTER), c).wait_recv()
             value = combined(OUTER, c, None)
+            if c == bchunks - 1:
+                for h in range(2):
+                    low, high = h * (tokens // 2), (h + 1) * (tokens // 2)
+                    rs_half(1, 1, h, to_in).wait_recv()
+                    total = value[low:high] + rin[1, c, low:high].astype(jnp.float32)
+                    part[2, c, low:high] = total.astype(jnp.bfloat16)
+                    rs_half(2, 0, h, to_out).start()
+                return
             rs_copy(1, 1, c, to_in).wait_recv()
             part[2, c] = (value + rin[1, c].astype(jnp.float32)).astype(jnp.bfloat16)
             rs_copy(2, 0, c, to_out).start()
@@ -444,7 +463,11 @@
             xb_from(lot(OWN), c).wait_recv()
             pre[c] = combined(OWN, c, None)
         for c in range(bchunks):
-            rs_copy(2, 0, c, to_near).wait_recv()
+            if c == bchunks - 1:
+                for h in range(2):
+                    rs_half(2, 0, h, to_near).wait_recv()
+            else:
+                rs_copy(2, 0, c, to_near).wait_recv()
             value = pre[c] + rin[0, c].astype(jnp.float32)
             out[:, bcols(c)] = value.astype(jnp.bfloat16)
 
@@ -495,7 +518,7 @@
             dma((4,)), dma((5, chunks)), dma((4,)),
             dma((5,)), dma((5, bchunks)),
             dma((4,)), dma((4, bchunks)),
-            dma((3,)), dma((2, bchunks)),
+            dma((3,)), dma((2, bchunks + 1)),
         ],
         compiler_params=pltpu.CompilerParams(
             collective_id=0, has_side_effects=True, vmem_limit_bytes=40 * 1024 * 1024

time: 61.6 us -> 61.1 us (level)
  no operation moved by 1% of the time
where the time goes in v5:
time: 61.1 us; the launch traced here: 60.9 us
  Pallas kernels  60.1 us (98%)
  local copies, waits for them, and re-layouts  0.8 us (1%)
    pallas_call x1, Pallas kernels, fused(): pl.pallas_call(functools.partial(kernel, n, m, cap, chunks, bchunks), out...  60.1 us

profile of v5, /device:TPU:0, one launch (start us, length us, event | category | flops | bytes accessed | tf_op | source)
XLA Modules:
  0.0 60.9 jit_solution(8165845959840979763)
XLA Ops:
  0.0 60.1 %experts.1 = bf16[128,2048]{1,0:T(8,128)(2,1)S(1)} custom-call(bf16[128,2048]{1,0:T(8,128)(2,1)} %hid_hbm.1, s32[2,128]{1,0:T(2,128)} %bitcast.4, f32[2,128]{1,0:T(2,128)} %bitcast.5, f32[1,2048]{1,0:T(1,128)} %bitcast.3, bf16[1,2048,512]{2,1,0:T(8,128)(2,1)} %gate_hbm.1, bf16[1,2048,512]{2,1,0:T(8,128)(2,1)} %up_hbm.1, bf16[1,512,2048]{2,1,0:T(8,128)(2,1)} %down_hbm.1), custom_call_target="tpu_custom_call" | custom-call | tf_op jit(solution)/shard_map/experts/pallas_call | solution.py:495
  60.1 0.8 %copy.9 = bf16[128,2048]{1,0:T(8,128)(2,1)} copy(bf16[128,2048]{1,0:T(8,128)(2,1)S(1)} %experts.1) | data formatting | bytes 1048576
